TPU v7x, 32 devices: a whole 2x2x4 slice. The times are simulated.
32 devices in a mesh: sp: 16 (over z, y, core), tp: 2 (over x).
Axes of the slice: x: 2, y: 2, z: 4, core: 2. Of those that a mesh axis runs over, the one named last changes fastest.
Arguments:
- tokens: bfloat16 [4096, 2048], P(('sp', 'tp')), may hold values from -6 to 6
- norm_gain: float32 [2048], replicated, may hold values from 0.1 to 1.9
- w_query: bfloat16 [2048, 1024], P('sp', 'tp'), may hold values from -0.125 to 0.125
- w_forget: bfloat16 [2048, 1024], P('sp', 'tp'), may hold values from -0.125 to 0.125
- w_input: bfloat16 [2048, 1024], P('sp', 'tp'), may hold values from -0.125 to 0.125
- w_outgate: bfloat16 [2048, 1024], P('sp', 'tp'), may hold values from -0.125 to 0.125
- w_bgate: bfloat16 [2048, 1024], P('sp', 'tp'), may hold values from -0.125 to 0.125
- w_cgate: bfloat16 [2048, 1024], P('sp', 'tp'), may hold values from -0.125 to 0.125
- w_value: bfloat16 [2048, 1024], P('sp', 'tp'), may hold values from -0.125 to 0.125
- floor_gap: float32 [8, 128], P('tp'), may hold values from 0 to 0.06
- extra_decay: float32 [4096, 8], P('sp', 'tp'), may hold values from -1 to 0
- start_state: float32 [8, 128, 128], P('tp'), may hold values from -0.109375 to 0.109375
- state_gain: float32 [128], replicated, may hold values from 0.1 to 1.9
- conv_taps: float32 [3, 1024], P(None, 'tp'), may hold values from -3 to 3
- out_rec: bfloat16 [1024, 2048], P('tp', 'sp'), may hold values from -0.125 to 0.125
- out_conv: bfloat16 [1024, 2048], P('tp', 'sp'), may hold values from -0.125 to 0.125
Outputs:
- mixed_sum: bfloat16 [4096, 2048], P(('sp', 'tp'))
All inputs are finite; a program needn't handle non-finite values.
Results may differ from a plain program's by a relative error of at most 0.018.
Values may be sent and summed in bfloat16 or wider, within the bound.
A program may use at most 64 MiB of HBM per device.

v0:
```python
import jax
import jax.numpy as jnp
from jax import lax
from jax.sharding import PartitionSpec as P

BLOCK = 64
eps = 1e-06
highest_precision = lax.Precision.HIGHEST


def prefix(value, axis, join, neutral):
    count, mine = (lax.axis_size(axis), lax.axis_index(axis))
    pieces = jax.tree.map(lambda part: lax.all_gather(part, axis), value)
    so_far = jax.tree.map(
        lambda part, zero: jnp.full_like(part, 0) + jnp.asarray(zero, part.dtype), value, neutral
    )

    def hop(position, so_far):
        longer = join(so_far, jax.tree.map(lambda part: part[position], pieces))
        return jax.tree.map(lambda new, old: jnp.where(position < mine, new, old), longer, so_far)

    return lax.fori_loop(0, count - 1, hop, so_far)


def shifted(block, axis, distance):
    devices = range(lax.axis_size(axis))
    route = [(i - distance, i) for i in devices if i - distance in devices]
    return lax.ppermute(block, axis, route)


def rms_scale(values):
    return lax.rsqrt(jnp.mean(values * values, axis=-1, keepdims=True) + eps)


def local_blocks(queries, write_in, inputs, log_keep, block_len):
    length, head_count, address_feature_count = queries.shape
    value_dim = inputs.shape[-1]
    blocks_count = length // block_len

    def blocked(tensor):
        return tensor.reshape(blocks_count, block_len, head_count, tensor.shape[-1]).transpose(
            0, 2, 1, 3
        )

    def unblock(tensor):
        return tensor.transpose(0, 2, 1, 3).reshape(length, head_count, tensor.shape[-1])

    causal = (jnp.arange(block_len)[:, None] >= jnp.arange(block_len)[None, :])[None, :, :, None]

    def advance(carried, pieces):
        memory_state, offset = carried
        query_block, write_blk, input_block, keep_blk = pieces
        running_state = jnp.cumsum(keep_blk, axis=1)
        spread = running_state[:, :, None, :] - running_state[:, None, :, :]
        decays = jnp.where(causal, jnp.exp(jnp.minimum(spread, 0.0)), 0.0)
        scores = jnp.sum(query_block[:, :, None, :] * write_blk[:, None, :, :] * decays, axis=-1)
        final_output = jnp.einsum(
            "qcp,qpi->qci",
            query_block * jnp.exp(running_state),
            memory_state,
            precision=highest_precision,
        )
        final_output = final_output + jnp.einsum(
            "hts,hsv->htv", scores, input_block, precision=highest_precision
        )
        lifted_state = query_block * jnp.exp(running_state + offset[:, None, :])
        final_state = running_state[:, -1, :]
        weighted_value = write_blk * jnp.exp(final_state[:, None, :] - running_state)
        memory_state = memory_state * jnp.exp(final_state)[:, :, None] + jnp.einsum(
            "euz,eul->ezl", weighted_value, input_block, precision=highest_precision
        )
        return ((memory_state, offset + final_state), (final_output, lifted_state))

    initial = (
        jnp.zeros((head_count, address_feature_count, value_dim), jnp.float32),
        jnp.zeros((head_count, address_feature_count), jnp.float32),
    )
    finals, outputs = lax.scan(
        advance, initial, (blocked(queries), blocked(write_in), blocked(inputs), blocked(log_keep))
    )
    return (unblock(outputs[0]), unblock(outputs[1]), finals[0], jnp.exp(finals[1]))


def chain(earlier, later):
    return (earlier[0] * later[0], earlier[1] * later[0][:, :, None] + later[1])


def on_device(
    tokens,
    norm_gain,
    w_query,
    w_forget,
    w_input,
    w_outgate,
    w_bgate,
    w_cgate,
    w_value,
    floor_gap,
    extra_decay,
    start_state,
    state_gain,
    conv_taps,
    out_rec,
    out_conv,
):
    tokens_f = tokens.astype(jnp.float32)
    normed = (tokens_f * rms_scale(tokens_f) * norm_gain).astype(jnp.bfloat16)
    weights = (w_query, w_forget, w_input, w_outgate, w_bgate, w_cgate, w_value)
    whole_weights = (
        lax.all_gather(w_query, "sp", axis=0, tiled=True),
        lax.all_gather(w_forget, "sp", axis=0, tiled=True),
        lax.all_gather(w_input, "sp", axis=0, tiled=True),
        lax.all_gather(w_outgate, "sp", axis=0, tiled=True),
        lax.all_gather(w_bgate, "sp", axis=0, tiled=True),
        lax.all_gather(w_cgate, "sp", axis=0, tiled=True),
        lax.all_gather(w_value, "sp", axis=0, tiled=True),
    )

    def project(shard_rows):
        return jnp.concatenate(
            [
                jnp.dot(shard_rows, matrix, preferred_element_type=jnp.float32).astype(jnp.bfloat16)
                for matrix in whole_weights
            ],
            axis=1,
        )

    joined = project(lax.all_gather(normed, "tp", axis=0, tiled=True))
    borders = [0]
    for matrix in weights:
        borders.append(borders[-1] + matrix.shape[1])
    projected = [joined[:, borders[number] : borders[number + 1]] for number in range(len(weights))]
    query_raw, forget_raw, input_raw, outgate_raw, bgate_raw, cgate_raw, value_raw = projected
    length = query_raw.shape[0]
    head_count, address_feature_count = floor_gap.shape
    value_dim = start_state.shape[2]
    queries = jax.nn.silu(query_raw.astype(jnp.float32)).reshape(
        length, head_count, address_feature_count
    )
    write_in = floor_gap[None] * jax.nn.sigmoid(-forget_raw.astype(jnp.float32)).reshape(
        length, head_count, address_feature_count
    )
    log_keep = jnp.log1p(-write_in) + extra_decay[:, :, None]
    inputs = input_raw.astype(jnp.float32).reshape(length, head_count, value_dim)
    output_list, lifted_state, memory_state, kept = local_blocks(
        queries, write_in, inputs, log_keep, BLOCK
    )
    before_keep, before_memory = prefix(
        (kept, memory_state), "sp", chain, (jnp.ones_like(kept), jnp.zeros_like(memory_state))
    )
    carried_hidden_prior = start_state * before_keep[:, :, None] + before_memory
    blended_state = output_list + jnp.einsum(
        "sqa,qar->sqr", lifted_state, carried_hidden_prior, precision=highest_precision
    )
    gate_out = jax.nn.silu(outgate_raw.astype(jnp.float32)).reshape(length, head_count, value_dim)
    rec_out = (
        (blended_state * rms_scale(blended_state) * state_gain * gate_out)
        .reshape(length, head_count * value_dim)
        .astype(jnp.bfloat16)
    )
    rim_rows = jnp.stack([cgate_raw[length - 2 :], value_raw[length - 2 :]])
    before_rim = shifted(rim_rows, "sp", 1)
    convolution_gate_widened = jnp.concatenate([before_rim[0], cgate_raw], axis=0).astype(
        jnp.float32
    )
    value_ext = jnp.concatenate([before_rim[1], value_raw], axis=0).astype(jnp.float32)
    gated = convolution_gate_widened * value_ext
    conv_out = (
        conv_taps[0] * gated[:length]
        + conv_taps[1] * gated[1 : length + 1]
        + conv_taps[2] * gated[2:]
    )
    short_out = (bgate_raw.astype(jnp.float32) * conv_out).astype(jnp.bfloat16)
    rec_weight, conv_weight = (
        lax.all_gather(out_rec, "sp", axis=1, tiled=True),
        lax.all_gather(out_conv, "sp", axis=1, tiled=True),
    )
    product = jnp.dot(rec_out, rec_weight, preferred_element_type=jnp.float32)
    return lax.psum_scatter(
        (product + jnp.dot(short_out, conv_weight, preferred_element_type=jnp.float32)).astype(
            jnp.bfloat16
        ),
        "tp",
        scatter_dimension=0,
        tiled=True,
    )


def solution(mesh):
    placed = (
        P(("sp", "tp"), None),
        P(),
        P("sp", "tp"),
        P("sp", "tp"),
        P("sp", "tp"),
        P("sp", "tp"),
        P("sp", "tp"),
        P("sp", "tp"),
        P("sp", "tp"),
        P("tp", None),
        P("sp", "tp"),
        P("tp", None, None),
        P(),
        P(None, "tp"),
        P("tp", "sp"),
        P("tp", "sp"),
    )
    return jax.shard_map(
        on_device, mesh=mesh, in_specs=placed, out_specs=P(("sp", "tp"), None), check_vma=False
    )
```

profile of v0, /device:TPU:0, one launch (start us, length us, event | category | flops | bytes accessed | tf_op | source)
XLA Modules:
  0.0 498.2 jit_solution(12257426766689084749)
XLA Ops:
  6.5 1.2 fusion.37
  7.8 2.0 fusion.39
  14.0 20.0 %all-gather.15.cloned.1.call-done = bf16[256,2048]{1,0:T(8,128)(2,1)} async-done(((bf16[128,2048]{1,0:T(8,128)(2,1)}), bf16[256,2048]{1,0:T(8,128)(2,1)}) %all-gather.15.cloned.1.call-update) | async-done | bytes 1048592 | tf_op jit(solution)/shard_map/all_gather | solution.py:128
  34.0 43.6 %all-gather.19.cloned.1.call-done = bf16[2048,512]{1,0:T(8,128)(2,1)} async-done(((bf16[128,512]{1,0:T(8,128)(2,1)}), bf16[2048,512]{1,0:T(8,128)(2,1)}) %all-gather.19.cloned.1.call-update) | async-done | bytes 2097168 | tf_op jit(solution)/shard_map/all_gather | solution.py:112
  77.7 2.6 fusion.31
  80.5 39.6 %all-gather.21.cloned.1.call-done = bf16[2048,512]{1,0:T(8,128)(2,1)} async-done(((bf16[128,512]{1,0:T(8,128)(2,1)}), bf16[2048,512]{1,0:T(8,128)(2,1)}) %all-gather.21.cloned.1.call-update) | async-done | bytes 2097168 | tf_op jit(solution)/shard_map/all_gather | solution.py:110
  120.0 2.4 divide_multiply_fusion.1
  122.6 39.7 %all-gather.17.cloned.1.call-done = bf16[2048,512]{1,0:T(8,128)(2,1)} async-done(((bf16[128,512]{1,0:T(8,128)(2,1)}), bf16[2048,512]{1,0:T(8,128)(2,1)}) %all-gather.17.cloned.1.call-update) | async-done | bytes 2097168 | tf_op jit(solution)/shard_map/all_gather | solution.py:111
  162.2 3.2 fusion.30
  165.4 1.2 reshape.81
  167.0 22.6 %while.33 = (s32[]{:T(128)}, f32[4,128,128]{2,1,0:T(8,128)S(1)}, f32[4,128]{1,0:T(4,128)S(1)}, f32[4,4,64,128]{3,2,0,1:T(8,128)}, f32[4,4,64,128]{3,2,0,1:T(8,12...) while((s32[]{:T(128)}, f32[4,128,128]{2,1,0:T(8,128)S(1)}, ...), condition=%wide.region_4.5_spmd.clone, body=%wide.region_1.4_spmd.clone.sunk | while | flops 140923904 | bytes 4028565 | solution.py:78
  167.3 3.4 multiply_reduce_fusion.3
  172.9 3.4 multiply_reduce_fusion.3
  178.6 3.4 multiply_reduce_fusion.3
  184.2 3.4 multiply_reduce_fusion.3
  192.6 11.9 %all-gather.31.cloned.1.call-done = bf16[2048,512]{1,0:T(8,128)(2,1)} async-done(((bf16[128,512]{1,0:T(8,128)(2,1)}), bf16[2048,512]{1,0:T(8,128)(2,1)}) %all-gather.31.cloned.1.call-update) | async-done | bytes 2097168 | tf_op jit(solution)/shard_map/all_gather | solution.py:116
  204.5 2.6 convolution_convert_fusion
  207.1 39.6 %all-gather.29.cloned.1.call-done = bf16[2048,512]{1,0:T(8,128)(2,1)} async-done(((bf16[128,512]{1,0:T(8,128)(2,1)}), bf16[2048,512]{1,0:T(8,128)(2,1)}) %all-gather.29.cloned.1.call-update) | async-done | bytes 2097168 | tf_op jit(solution)/shard_map/all_gather | solution.py:115
  246.7 2.3 convolution_convert_fusion.1
  249.1 2.3 collective-permute-start
  251.3 37.7 %all-gather.23.cloned.1.call-done = bf16[2048,512]{1,0:T(8,128)(2,1)} async-done(((bf16[128,512]{1,0:T(8,128)(2,1)}), bf16[2048,512]{1,0:T(8,128)(2,1)}) %all-gather.23.cloned.1.call-update) | async-done | bytes 2097168 | tf_op jit(solution)/shard_map/all_gather | solution.py:113
  289.1 3.2 divide_multiply_fusion
  292.2 19.4 %all-gather.2 = f32[16,4,128]{2,1,0:T(4,128)S(1)} all-gather(f32[1,4,128]{2,1,0:T(4,128)S(1)} %exponential_bitcast_fusion), channel_id=2, replica_groups=mesh['sp'=16,'tp'=2] {'sp'}, dimensions={0}, use_global_device_ids=true | all-gather | bytes 34816 | tf_op jit(solution)/shard_map/all_gather | solution.py:13
  311.8 1.2 copy.52
  313.1 1.1 convert_multiply_fusion.2
  314.2 26.2 %all-gather.35.cloned.1.call-done = f32[64,128,128]{2,1,0:T(8,128)} async-done(((f32[4,128,128]{2,1,0:T(8,128)}), f32[64,128,128]{2,1,0:T(8,128)}) %all-gather.35.cloned.1.call-update) | async-done | bytes 4194320 | tf_op jit(solution)/shard_map/all_gather | solution.py:13
  340.4 18.0 %while.34 = (s32[]{:T(128)}, f32[4,128]{1,0:T(4,128)S(1)}, f32[4,128,128]{2,1,0:T(8,128)S(1)}, s32[]{:T(128)}, f32[16,4,128]{2,1,0:T(4,128)S(1)}, /*index=5*/f32[16,4,128,128]{3,2,1,0:T(8,128)}, s32[]{:T(128)}, s32[]{:T(128)}) while((s32[]{:T(128)}, f32[4,128]{1,0:T(4,128)S(1)}, f32[4,128,128]{2,1,0:T(8,128)S(1)}, s32[]{:T(128)}, ...), condition=%wide.region_6.7_spmd.clone, body=%wide.region_5.6_spmd.clone.sunk | while | flops 263684 | bytes 796787 | solution.py:22
  340.5 1.1 fusion.94
  341.7 1.2 fusion.94
  342.9 1.2 fusion.94
  344.1 1.2 fusion.94
  345.3 1.2 fusion.94
  346.5 1.2 fusion.94
  347.7 1.2 fusion.94
  348.9 1.2 fusion.94
  350.1 1.2 fusion.94
  351.3 1.2 fusion.94
  352.5 1.2 fusion.94
  353.7 1.2 fusion.94
  354.9 1.2 fusion.94
  356.1 1.2 fusion.94
  357.3 1.2 fusion.94
  359.4 22.9 %all-gather.25.cloned.1.call-done = bf16[512,2048]{1,0:T(8,128)(2,1)} async-done(((bf16[512,128]{1,0:T(8,128)(2,1)}), bf16[512,2048]{1,0:T(8,128)(2,1)}) %all-gather.25.cloned.1.call-update) | async-done | bytes 2097168 | tf_op jit(solution)/shard_map/all_gather | solution.py:175
  382.2 2.3 fusion.53
  384.5 40.3 %all-gather.27.cloned.1.call-done = bf16[2048,512]{1,0:T(8,128)(2,1)} async-done(((bf16[128,512]{1,0:T(8,128)(2,1)}), bf16[2048,512]{1,0:T(8,128)(2,1)}) %all-gather.27.cloned.1.call-update) | async-done | bytes 2097168 | tf_op jit(solution)/shard_map/all_gather | solution.py:114
  424.8 42.0 %all-gather.33.cloned.1.call-done = bf16[512,2048]{1,0:T(8,128)(2,1)} async-done(((bf16[512,128]{1,0:T(8,128)(2,1)}), bf16[512,2048]{1,0:T(8,128)(2,1)}) %all-gather.33.cloned.1.call-update) | async-done | bytes 2097168 | tf_op jit(solution)/shard_map/all_gather | solution.py:176
  466.7 4.9 fusion.25
  471.7 19.6 %reduce-scatter.2.cloned.1.call-done = bf16[128,2048]{1,0:T(8,128)(2,1)} async-done(((bf16[256,2048]{1,0:T(8,128)(2,1)}), bf16[128,2048]{1,0:T(8,128)(2,1)}) %reduce-scatter.2.cloned.1.call-update) | async-done | bytes 524304 | tf_op jit(solution)/shard_map/reduce_scatter | solution.py:179
  (123 shorter events, 17.7 us)
Async XLA Ops:
  6.5 7.4 %copy-start.7 = (f32[256,4]{0,1:T(4,128)S(1)}, f32[256,4]{0,1:T(4,128)}, u32[]{:S(2)}) copy-start(f32[256,4]{0,1:T(4,128)} %param.30) | copy-start | bytes 12292
  6.5 27.5 %all-gather.15.cloned.1.call-start = ((), (), s32[]{:S(2)}) async-start(), calls=%async_computation.1 | async-start | bytes 1572864 | tf_op jit(solution)/shard_map/all_gather | solution.py:128
  9.8 67.8 %all-gather.19.cloned.1.call-start = ((), (), s32[]{:S(2)}) async-start(), calls=%async_computation.3 | async-start | bytes 2228224 | tf_op jit(solution)/shard_map/all_gather | solution.py:112
  10.6 109.4 %all-gather.21.cloned.1.call-start = ((), (), s32[]{:S(2)}) async-start(), calls=%async_computation.4 | async-start | bytes 2228224 | tf_op jit(solution)/shard_map/all_gather | solution.py:110
  11.3 150.9 %all-gather.17.cloned.1.call-start = ((), (), s32[]{:S(2)}) async-start(), calls=%async_computation.2 | async-start | bytes 2228224 | tf_op jit(solution)/shard_map/all_gather | solution.py:111
  11.9 192.6 %all-gather.31.cloned.1.call-start = ((), (), s32[]{:S(2)}) async-start(), calls=%async_computation.9 | async-start | bytes 2228224 | tf_op jit(solution)/shard_map/all_gather | solution.py:116
  12.5 234.2 %all-gather.29.cloned.1.call-start = ((), (), s32[]{:S(2)}) async-start(), calls=%async_computation.8 | async-start | bytes 2228224 | tf_op jit(solution)/shard_map/all_gather | solution.py:115
  13.1 276.0 %all-gather.23.cloned.1.call-start = ((), (), s32[]{:S(2)}) async-start(), calls=%async_computation.5 | async-start | bytes 2228224 | tf_op jit(solution)/shard_map/all_gather | solution.py:113
  13.8 326.6 %all-gather.35.cloned.1.call-start = ((), (), s32[]{:S(2)}) async-start(), calls=%async_computation.12 | async-start | bytes 4456448 | tf_op jit(solution)/shard_map/all_gather | solution.py:13
  34.0 86.0 %copy-start.1 = (bf16[256,2048]{1,0:T(8,128)(2,1)S(1)}, bf16[256,2048]{1,0:T(8,128)(2,1)}, u32[]{:S(2)}) copy-start(bf16[256,2048]{1,0:T(8,128)(2,1)} %all-gather.15.cloned.1.call-done) | copy-start | bytes 3145732
  165.4 1.4 copy-start.8
  167.0 25.5 %copy-start.6 = (f32[3,512]{1,0:T(4,128)S(1)}, f32[3,512]{1,0:T(4,128)}, u32[]{:S(2)}) copy-start(f32[3,512]{1,0:T(4,128)} %param.33) | copy-start | bytes 18436
  189.7 0.7 copy-start
  190.4 56.3 %copy-start.2 = (bf16[256,2048]{1,0:T(8,128)(2,1)S(1)}, bf16[256,2048]{1,0:T(8,128)(2,1)}, u32[]{:S(2)}) copy-start(bf16[256,2048]{1,0:T(8,128)(2,1)} %all-gather.15.cloned.1.call-done) | copy-start | bytes 3145732
  190.4 191.8 %all-gather.25.cloned.1.call-start = ((), (), s32[]{:S(2)}) async-start(), calls=%async_computation.6 | async-start | bytes 2228224 | tf_op jit(solution)/shard_map/all_gather | solution.py:175
  191.1 233.7 %all-gather.27.cloned.1.call-start = ((), (), s32[]{:S(2)}) async-start(), calls=%async_computation.7 | async-start | bytes 2228224 | tf_op jit(solution)/shard_map/all_gather | solution.py:114
  191.7 275.0 %all-gather.33.cloned.1.call-start = ((), (), s32[]{:S(2)}) async-start(), calls=%async_computation.10 | async-start | bytes 2228224 | tf_op jit(solution)/shard_map/all_gather | solution.py:176
  192.5 298.9 %reduce-scatter.2.cloned.1.call-start = ((), (), s32[]{:S(2)}) async-start(), calls=%async_computation.11 | async-start | bytes 1572864 | tf_op jit(solution)/shard_map/reduce_scatter | solution.py:179
  249.0 43.2 %copy-start.4 = (bf16[256,512]{1,0:T(8,128)(2,1)}, bf16[256,512]{1,0:T(8,128)(2,1)S(1)}, u32[]{:S(2)}) copy-start(bf16[256,512]{1,0:T(8,128)(2,1)S(1)} %convolution_convert_fusion.1) | copy-start | bytes 786436
  249.0 62.6 %copy-start.3 = (f32[4,4,64,128]{3,2,0,1:T(8,128)S(1)}, f32[4,4,64,128]{3,2,0,1:T(8,128)}, u32[]{:S(2)}) copy-start(f32[4,4,64,128]{3,2,0,1:T(8,128)} %get-tuple-element.170) | copy-start | bytes 1572868
  249.1 64.0 %collective-permute-start = (bf16[2,2,512]{2,1,0:T(2,128)(2,1)S(1)}, bf16[2,2,512]{2,1,0:T(2,128)(2,1)S(1)}, u32[]{:S(2)}, u32[]{:S(2)}) collective-permute-start(bf16[2,2,512]{2,1,0:T(2,128)(2,1)S(1)} %pad_maximum_fusion), channel_id=1, source_target_pairs={{0,2},{2,4},{4,6},{6,8},{8,10},{10,12},{12,14},{14,16},{16,18},{18... | collective-permute-start | bytes 12296 | tf_op jit(solution)/shard_map/ppermute | solution.py:28
  314.2 44.2 %copy-start.5 = (f32[4,128,128]{2,1,0:T(8,128)S(1)}, f32[4,128,128]{2,1,0:T(8,128)}, u32[]{:S(2)}) copy-start(f32[4,128,128]{2,1,0:T(8,128)} %param.31) | copy-start | bytes 786436
  358.4 0.8 copy-start.9
Sparse Core Ops, SparseCore 0:
  10.0 23.9 all-gather.14
  36.2 41.4 all-gather.18
  79.8 40.1 all-gather.20
  122.0 40.1 all-gather.16
  164.3 40.1 all-gather.30
  206.5 40.1 all-gather.28
  248.9 40.1 all-gather.22
  291.2 49.1 all-gather.34
  342.6 39.5 all-gather.24
  384.2 40.5 all-gather.26
  427.0 39.7 all-gather.32
  471.8 19.4 reduce-scatter.1
where the time goes:
time: 499 us; the launch traced here: 498 us
  waiting for transfers between devices  389 us (78%)
  other arithmetic  36.6 us (7%)
  matrix products  32 us (6%)
  blocking collectives  19.4 us (4%)
  between operations  13.9 us (3%)
    all_gather x1, waiting for transfers between devices, on_device(): lax.all_gather(w_input, 'sp', axis=0, tiled=True)  43.6 us
    all_gather x1, waiting for transfers between devices, on_device(): lax.all_gather(out_conv, 'sp', axis=1, tiled=True)  42 us
    all_gather x1, waiting for transfers between devices, on_device(): lax.all_gather(w_bgate, 'sp', axis=0, tiled=True)  40.3 us
    all_gather x1, waiting for transfers between devices, on_device(): lax.all_gather(w_forget, 'sp', axis=0, tiled=True)  39.7 us
    all_gather x1, waiting for transfers between devices, on_device(): lax.all_gather(w_cgate, 'sp', axis=0, tiled=True)  39.6 us
    all_gather x1, waiting for transfers between devices, on_device(): lax.all_gather(w_query, 'sp', axis=0, tiled=True)  39.6 us
    all_gather x1, waiting for transfers between devices, on_device(): lax.all_gather(w_outgate, 'sp', axis=0, tiled=True)  37.7 us
    all_gather x1, waiting for transfers between devices, prefix(): pieces = jax.tree.map(lambda part: lax.all_gather(part, axis), value)  26.2 us
  transfers between devices with their start and end apart: 13, of which 12 were waited for; matrix products, arithmetic and copies ran while one was open for 13% of the time, Pallas kernels for 0%

commit v1 on v0

--- a/solution.py
+++ b/solution.py
@@ -109,7 +109,9 @@
     whole_weights = (
         lax.all_gather(w_query, "sp", axis=0, tiled=True),
         lax.all_gather(w_forget, "sp", axis=0, tiled=True),
-        lax.all_gather(w_input, "sp", axis=0, tiled=True),
+        jnp.concatenate(
+            lax.all_to_all(jnp.stack([w_input] * lax.axis_size("sp")), "sp", 0, 0), axis=0
+        ),
         lax.all_gather(w_outgate, "sp", axis=0, tiled=True),
         lax.all_gather(w_bgate, "sp", axis=0, tiled=True),
         lax.all_gather(w_cgate, "sp", axis=0, tiled=True),

time: 499 us -> 467 us (0.936)
  waiting for transfers between devices: 389 us -> 348 us
  starting transfers between devices: 2.69 us -> 10.2 us
    all_gather x1 -> x0, waiting for transfers between devices: 43.6 us -> none  [on_device(): lax.all_gather(w_input, 'sp', axis=0, tiled=True)]
    all_to_all x0 -> x1, waiting for transfers between devices: none -> 32.9 us  [on_device(): lax.all_to_all(jnp.stack([w_input] * lax.axis_size('sp')), 'sp', 0, 0)]
    all_gather x1, waiting for transfers between devices: 39.6 us -> 16.2 us  [on_device(): lax.all_gather(w_query, 'sp', axis=0, tiled=True)]
    all_gather x1, waiting for transfers between devices: 20 us -> 11.6 us  [on_device(): joined = project(lax.all_gather(normed, 'tp', axis=0, tiled=True))]
    all_to_all x0 -> x1, starting transfers between devices: none -> 7.55 us  [on_device(): lax.all_to_all(jnp.stack([w_input] * lax.axis_size('sp')), 'sp', 0, 0)]
  transfers between devices with their start and end apart: 13 -> 13, of which waited for: 12 -> 12; matrix products, arithmetic and copies ran while one was open for 13% -> 14% of each run, Pallas kernels for 0% -> 0%
where the time goes in v1:
time: 467 us; the launch traced here: 466 us
  waiting for transfers between devices  348 us (75%)
  other arithmetic  36.6 us (8%)
  matrix products  31.4 us (7%)
  blocking collectives  19.4 us (4%)
  between operations  13.6 us (3%)
  starting transfers between devices  10.2 us (2%)
  local copies, waits for them, and re-layouts  6.48 us (1%)
    all_gather x1, waiting for transfers between devices, on_device(): lax.all_gather(out_conv, 'sp', axis=1, tiled=True)  41.8 us
    all_gather x1, waiting for transfers between devices, on_device(): lax.all_gather(w_forget, 'sp', axis=0, tiled=True)  41 us
    all_gather x1, waiting for transfers between devices, on_device(): lax.all_gather(w_bgate, 'sp', axis=0, tiled=True)  40.4 us
    all_gather x1, waiting for transfers between devices, on_device(): lax.all_gather(w_cgate, 'sp', axis=0, tiled=True)  39.6 us
    all_gather x1, waiting for transfers between devices, on_device(): lax.all_gather(w_outgate, 'sp', axis=0, tiled=True)  37.6 us
    all_to_all x1, waiting for transfers between devices, on_device(): lax.all_to_all(jnp.stack([w_input] * lax.axis_size('sp')), 'sp', 0, 0)  32.9 us
    all_gather x1, waiting for transfers between devices, prefix(): pieces = jax.tree.map(lambda part: lax.all_gather(part, axis), value)  26.2 us
    all_gather x1, waiting for transfers between devices, on_device(): lax.all_gather(out_rec, 'sp', axis=1, tiled=True)  22.9 us
  transfers between devices with their start and end apart: 13, of which 12 were waited for; matrix products, arithmetic and copies ran while one was open for 14% of the time, Pallas kernels for 0%

profile of v1, /device:TPU:0, one launch (start us, length us, event | category | flops | bytes accessed | tf_op | source)
XLA Modules:
  0.0 466.3 jit_solution(9486304590346292088)
XLA Ops:
  6.5 1.3 fusion.37
  7.8 2.0 fusion.39
  12.5 1.6 stack.8
  14.1 7.5 %all-to-all-start = ((bf16[16,128,512]{2,1,0:T(8,128)(2,1)}), bf16[16,128,512]{2,1,0:T(8,128)(2,1)S(1)}, u32[]{:S(2)}, u32[]{:S(2)}) async-start(bf16[16,128,512]{2,1,0:T(8,128)(2,1)} %stack.8), calls=%async_computation | async-start | bytes 4194304 | tf_op jit(solution)/shard_map/all_to_all | solution.py:113
  22.4 11.6 %all-gather.14.cloned.1.call-done = bf16[256,2048]{1,0:T(8,128)(2,1)} async-done(((bf16[128,2048]{1,0:T(8,128)(2,1)}), bf16[256,2048]{1,0:T(8,128)(2,1)}) %all-gather.14.cloned.1.call-update) | async-done | bytes 1048592 | tf_op jit(solution)/shard_map/all_gather | solution.py:130
  34.0 32.9 %all-to-all-done = bf16[16,128,512]{2,1,0:T(8,128)(2,1)S(1)} async-done(((bf16[16,128,512]{2,1,0:T(8,128)(2,1)}), bf16[16,128,512]{2,1,0:T(8,128)(2,1)S(1)}, u32[]{:S(2)}, u32[]{:S(2)}) %all-to-all-start) | async-done | bytes 2097184 | tf_op jit(solution)/shard_map/all_to_all | solution.py:113
  66.9 2.8 fusion.31
  69.7 1.3 reshape.91
  71.0 16.2 %all-gather.18.cloned.1.call-done = bf16[2048,512]{1,0:T(8,128)(2,1)} async-done(((bf16[128,512]{1,0:T(8,128)(2,1)}), bf16[2048,512]{1,0:T(8,128)(2,1)}) %all-gather.18.cloned.1.call-update) | async-done | bytes 2097168 | tf_op jit(solution)/shard_map/all_gather | solution.py:110
  87.2 2.4 divide_multiply_fusion.1
  89.7 41.0 %all-gather.16.cloned.1.call-done = bf16[2048,512]{1,0:T(8,128)(2,1)} async-done(((bf16[128,512]{1,0:T(8,128)(2,1)}), bf16[2048,512]{1,0:T(8,128)(2,1)}) %all-gather.16.cloned.1.call-update) | async-done | bytes 2097168 | tf_op jit(solution)/shard_map/all_gather | solution.py:111
  130.8 2.4 fusion.30
  134.4 22.6 %while.33 = (s32[]{:T(128)}, f32[4,128,128]{2,1,0:T(8,128)S(1)}, f32[4,128]{1,0:T(4,128)S(1)}, f32[4,4,64,128]{3,2,0,1:T(8,128)}, f32[4,4,64,128]{3,2,0,1:T(8,12...) while((s32[]{:T(128)}, f32[4,128,128]{2,1,0:T(8,128)S(1)}, ...), condition=%wide.region_4.5_spmd.clone, body=%wide.region_1.4_spmd.clone.sunk | while | flops 140923904 | bytes 4028565 | solution.py:78
  134.6 3.4 multiply_reduce_fusion.3
  140.2 3.4 multiply_reduce_fusion.3
  145.9 3.4 multiply_reduce_fusion.3
  151.5 3.4 multiply_reduce_fusion.3
  159.9 13.2 %all-gather.28.cloned.1.call-done = bf16[2048,512]{1,0:T(8,128)(2,1)} async-done(((bf16[128,512]{1,0:T(8,128)(2,1)}), bf16[2048,512]{1,0:T(8,128)(2,1)}) %all-gather.28.cloned.1.call-update) | async-done | bytes 2097168 | tf_op jit(solution)/shard_map/all_gather | solution.py:118
  173.0 2.6 convolution_convert_fusion
  175.7 39.6 %all-gather.26.cloned.1.call-done = bf16[2048,512]{1,0:T(8,128)(2,1)} async-done(((bf16[128,512]{1,0:T(8,128)(2,1)}), bf16[2048,512]{1,0:T(8,128)(2,1)}) %all-gather.26.cloned.1.call-update) | async-done | bytes 2097168 | tf_op jit(solution)/shard_map/all_gather | solution.py:117
  215.3 2.3 convolution_convert_fusion.1
  217.6 2.3 collective-permute-start
  219.9 37.6 %all-gather.20.cloned.1.call-done = bf16[2048,512]{1,0:T(8,128)(2,1)} async-done(((bf16[128,512]{1,0:T(8,128)(2,1)}), bf16[2048,512]{1,0:T(8,128)(2,1)}) %all-gather.20.cloned.1.call-update) | async-done | bytes 2097168 | tf_op jit(solution)/shard_map/all_gather | solution.py:115
  257.5 3.2 divide_multiply_fusion
  260.6 19.4 %all-gather.2 = f32[16,4,128]{2,1,0:T(4,128)S(1)} all-gather(f32[1,4,128]{2,1,0:T(4,128)S(1)} %exponential_bitcast_fusion), channel_id=2, replica_groups=mesh['sp'=16,'tp'=2] {'sp'}, dimensions={0}, use_global_device_ids=true | all-gather | bytes 34816 | tf_op jit(solution)/shard_map/all_gather | solution.py:13
  280.2 1.2 copy.52
  282.6 26.2 %all-gather.32.cloned.1.call-done = f32[64,128,128]{2,1,0:T(8,128)} async-done(((f32[4,128,128]{2,1,0:T(8,128)}), f32[64,128,128]{2,1,0:T(8,128)}) %all-gather.32.cloned.1.call-update) | async-done | bytes 4194320 | tf_op jit(solution)/shard_map/all_gather | solution.py:13
  308.9 18.0 %while.34 = (s32[]{:T(128)}, f32[4,128]{1,0:T(4,128)S(1)}, f32[4,128,128]{2,1,0:T(8,128)S(1)}, s32[]{:T(128)}, f32[16,4,128]{2,1,0:T(4,128)S(1)}, /*index=5*/f32[16,4,128,128]{3,2,1,0:T(8,128)}, s32[]{:T(128)}, s32[]{:T(128)}) while((s32[]{:T(128)}, f32[4,128]{1,0:T(4,128)S(1)}, f32[4,128,128]{2,1,0:T(8,128)S(1)}, s32[]{:T(128)}, ...), condition=%wide.region_6.7_spmd.clone, body=%wide.region_5.6_spmd.clone.sunk | while | flops 263684 | bytes 796787 | solution.py:22
  310.1 1.2 fusion.94
  311.3 1.2 fusion.94
  312.5 1.2 fusion.94
  313.7 1.2 fusion.94
  314.9 1.2 fusion.94
  316.1 1.2 fusion.94
  317.3 1.2 fusion.94
  318.5 1.2 fusion.94
  319.7 1.2 fusion.94
  320.9 1.2 fusion.94
  322.1 1.2 fusion.94
  323.3 1.2 fusion.94
  324.5 1.2 fusion.94
  325.7 1.2 fusion.94
  327.8 22.9 %all-gather.22.cloned.1.call-done = bf16[512,2048]{1,0:T(8,128)(2,1)} async-done(((bf16[512,128]{1,0:T(8,128)(2,1)}), bf16[512,2048]{1,0:T(8,128)(2,1)}) %all-gather.22.cloned.1.call-update) | async-done | bytes 2097168 | tf_op jit(solution)/shard_map/all_gather | solution.py:177
  350.6 2.3 fusion.53
  352.9 40.4 %all-gather.24.cloned.1.call-done = bf16[2048,512]{1,0:T(8,128)(2,1)} async-done(((bf16[128,512]{1,0:T(8,128)(2,1)}), bf16[2048,512]{1,0:T(8,128)(2,1)}) %all-gather.24.cloned.1.call-update) | async-done | bytes 2097168 | tf_op jit(solution)/shard_map/all_gather | solution.py:116
  393.3 41.8 %all-gather.30.cloned.1.call-done = bf16[512,2048]{1,0:T(8,128)(2,1)} async-done(((bf16[512,128]{1,0:T(8,128)(2,1)}), bf16[512,2048]{1,0:T(8,128)(2,1)}) %all-gather.30.cloned.1.call-update) | async-done | bytes 2097168 | tf_op jit(solution)/shard_map/all_gather | solution.py:178
  435.1 4.9 %fusion.25 = bf16[256,2048]{1,0:T(8,128)(2,1)} fusion(f32[256,2048]{1,0:T(8,128)S(1)} %fusion.53, bf16[512,2048]{1,0:T(8,128)(2,1)} %all-gather.30.cloned.1.call-done, bf16[256,2048]{1,0:T(8,128)(2,1)} %all-gather.14.cloned.1.call-done, bf16[2048,512]{1,0:T(8,128)(2,1)} %all-gather.24.cloned.1.call-done, f32[258,512]{1,0:T(8,128)S(1)} %convert_multiply_fusion.2, ...), kind=kOutput, calls=%fused_computation.38 | convolution fusion | flops 1075970048 | bytes 9967616 | tf_op jit(solution)/shard_map/dot_general | solution.py:182
  440.1 19.6 %reduce-scatter.2.cloned.1.call-done = bf16[128,2048]{1,0:T(8,128)(2,1)} async-done(((bf16[256,2048]{1,0:T(8,128)(2,1)}), bf16[128,2048]{1,0:T(8,128)(2,1)}) %reduce-scatter.2.cloned.1.call-update) | async-done | bytes 524304 | tf_op jit(solution)/shard_map/reduce_scatter | solution.py:181
  (127 shorter events, 19.8 us)
Async XLA Ops:
  6.5 6.0 %copy-start.7 = (bf16[128,512]{1,0:T(8,128)(2,1)S(1)}, bf16[128,512]{1,0:T(8,128)(2,1)}, u32[]{:S(2)}) copy-start(bf16[128,512]{1,0:T(8,128)(2,1)} %param.24) | copy-start | bytes 393220
  6.5 27.5 %all-gather.14.cloned.1.call-start = ((), (), s32[]{:S(2)}) async-start(), calls=%async_computation.2 | async-start | bytes 1572864 | tf_op jit(solution)/shard_map/all_gather | solution.py:130
  9.9 77.3 %all-gather.18.cloned.1.call-start = ((), (), s32[]{:S(2)}) async-start(), calls=%async_computation.4 | async-start | bytes 2228224 | tf_op jit(solution)/shard_map/all_gather | solution.py:110
  10.6 120.1 %all-gather.16.cloned.1.call-start = ((), (), s32[]{:S(2)}) async-start(), calls=%async_computation.3 | async-start | bytes 2228224 | tf_op jit(solution)/shard_map/all_gather | solution.py:111
  11.4 161.7 %all-gather.28.cloned.1.call-start = ((), (), s32[]{:S(2)}) async-start(), calls=%async_computation.9 | async-start | bytes 2228224 | tf_op jit(solution)/shard_map/all_gather | solution.py:118
  11.9 203.3 %all-gather.26.cloned.1.call-start = ((), (), s32[]{:S(2)}) async-start(), calls=%async_computation.8 | async-start | bytes 2228224 | tf_op jit(solution)/shard_map/all_gather | solution.py:117
  14.1 8.2 %copy-start.9 = (f32[256,4]{0,1:T(4,128)S(1)}, f32[256,4]{0,1:T(4,128)}, u32[]{:S(2)}) copy-start(f32[256,4]{0,1:T(4,128)} %param.30) | copy-start | bytes 12292
  14.1 52.8 %all-to-all-start = ((bf16[16,128,512]{2,1,0:T(8,128)(2,1)}), bf16[16,128,512]{2,1,0:T(8,128)(2,1)S(1)}, u32[]{:S(2)}, u32[]{:S(2)}) async-start(bf16[16,128,512]{2,1,0:T(8,128)(2,1)} %stack.8), calls=%async_computation | async-start | bytes 4194304 | tf_op jit(solution)/shard_map/all_to_all | solution.py:113
  21.7 235.8 %all-gather.20.cloned.1.call-start = ((), (), s32[]{:S(2)}) async-start(), calls=%async_computation.5 | async-start | bytes 2228224 | tf_op jit(solution)/shard_map/all_gather | solution.py:115
  22.3 286.6 %all-gather.32.cloned.1.call-start = ((), (), s32[]{:S(2)}) async-start(), calls=%async_computation.12 | async-start | bytes 4456448 | tf_op jit(solution)/shard_map/all_gather | solution.py:13
  66.9 20.3 %copy-start.1 = (bf16[256,2048]{1,0:T(8,128)(2,1)S(1)}, bf16[256,2048]{1,0:T(8,128)(2,1)}, u32[]{:S(2)}) copy-start(bf16[256,2048]{1,0:T(8,128)(2,1)} %all-gather.14.cloned.1.call-done) | copy-start | bytes 3145732
  133.1 0.7 copy-start.10
  133.3 1.0 copy-start.3
  134.4 25.4 %copy-start.8 = (f32[3,512]{1,0:T(4,128)S(1)}, f32[3,512]{1,0:T(4,128)}, u32[]{:S(2)}) copy-start(f32[3,512]{1,0:T(4,128)} %param.33) | copy-start | bytes 18436
  156.9 0.7 copy-start
  157.7 57.6 %copy-start.2 = (bf16[256,2048]{1,0:T(8,128)(2,1)S(1)}, bf16[256,2048]{1,0:T(8,128)(2,1)}, u32[]{:S(2)}) copy-start(bf16[256,2048]{1,0:T(8,128)(2,1)} %all-gather.14.cloned.1.call-done) | copy-start | bytes 3145732
  157.7 192.9 %all-gather.22.cloned.1.call-start = ((), (), s32[]{:S(2)}) async-start(), calls=%async_computation.6 | async-start | bytes 2228224 | tf_op jit(solution)/shard_map/all_gather | solution.py:177
  158.4 234.9 %all-gather.24.cloned.1.call-start = ((), (), s32[]{:S(2)}) async-start(), calls=%async_computation.7 | async-start | bytes 2228224 | tf_op jit(solution)/shard_map/all_gather | solution.py:116
  159.2 276.0 %all-gather.30.cloned.1.call-start = ((), (), s32[]{:S(2)}) async-start(), calls=%async_computation.10 | async-start | bytes 2228224 | tf_op jit(solution)/shard_map/all_gather | solution.py:178
  159.7 300.0 %reduce-scatter.2.cloned.1.call-start = ((), (), s32[]{:S(2)}) async-start(), calls=%async_computation.11 | async-start | bytes 1572864 | tf_op jit(solution)/shard_map/reduce_scatter | solution.py:181
  217.5 43.1 %copy-start.5 = (bf16[256,512]{1,0:T(8,128)(2,1)}, bf16[256,512]{1,0:T(8,128)(2,1)S(1)}, u32[]{:S(2)}) copy-start(bf16[256,512]{1,0:T(8,128)(2,1)S(1)} %convolution_convert_fusion.1) | copy-start | bytes 786436
  217.6 62.5 %copy-start.4 = (f32[4,4,64,128]{3,2,0,1:T(8,128)S(1)}, f32[4,4,64,128]{3,2,0,1:T(8,128)}, u32[]{:S(2)}) copy-start(f32[4,4,64,128]{3,2,0,1:T(8,128)} %get-tuple-element.170) | copy-start | bytes 1572868
  217.6 63.9 %collective-permute-start = (bf16[2,2,512]{2,1,0:T(2,128)(2,1)S(1)}, bf16[2,2,512]{2,1,0:T(2,128)(2,1)S(1)}, u32[]{:S(2)}, u32[]{:S(2)}) collective-permute-start(bf16[2,2,512]{2,1,0:T(2,128)(2,1)S(1)} %pad_maximum_fusion), channel_id=1, source_target_pairs={{0,2},{2,4},{4,6},{6,8},{8,10},{10,12},{12,14},{14,16},{16,18},{18... | collective-permute-start | bytes 12296 | tf_op jit(solution)/shard_map/ppermute | solution.py:28
  282.6 44.2 %copy-start.6 = (f32[4,128,128]{2,1,0:T(8,128)S(1)}, f32[4,128,128]{2,1,0:T(8,128)}, u32[]{:S(2)}) copy-start(f32[4,128,128]{2,1,0:T(8,128)} %param.31) | copy-start | bytes 786436
  326.8 0.8 copy-start.11
Sparse Core Ops, SparseCore 0:
  10.0 23.9 all-gather.13
  36.2 50.9 all-gather.17
  89.3 41.3 all-gather.15
  132.8 40.2 all-gather.27
  175.0 40.1 all-gather.25
  217.3 40.1 all-gather.19
  259.6 49.1 all-gather.31
  311.0 39.5 all-gather.21
  352.8 40.5 all-gather.23
  395.4 39.7 all-gather.29
  440.2 19.4 reduce-scatter.1
